TPU v7x, 256 devices: a whole 4x4x8 slice. The times are simulated.
256 devices in a mesh: ra: 32 (over z, y), cb: 8 (over x, core).
Axes of the slice: x: 4, y: 4, z: 8, core: 2. Of those that a mesh axis runs over, the one named last changes fastest.
Arguments:
- tokens: bfloat16 [2048, 16384], P('ra'), may hold values from -16 to 16
- norm_gain: float32 [2, 2048], replicated, may hold values from 0.1 to 1.9
- up_weight: float32 [2, 2048, 6144], P(None, 'ra', 'cb'), may hold values from -0.125 to 0.125
- gate_weight: float32 [2, 2048, 6144], P(None, 'ra', 'cb'), may hold values from -0.125 to 0.125
- up_scale: float32 [2, 6144], P(None, 'cb'), may hold values from 0.5 to 2
- gate_scale: float32 [2, 6144], P(None, 'cb'), may hold values from 0.5 to 2
- up_taps: float32 [2, 3, 6144], P(None, None, 'cb'), may hold values from -3 to 3
- gate_taps: float32 [2, 3, 6144], P(None, None, 'cb'), may hold values from -3 to 3
- down_weight: float32 [2, 2048, 6144], P(None, 'ra', 'cb'), may hold values from -0.078125 to 0.078125
- down_scale: float32 [2, 2048], replicated, may hold values from 0.5 to 2
Outputs:
- mixed: bfloat16 [2048, 16384], P('ra')
All inputs are finite; a program needn't handle non-finite values.
Results may differ from a plain program's by a relative error of at most 0.024.
Values may be sent and summed in bfloat16 or wider, within the bound.
No kernel may reach another device: no remote copies, remote signals or barrier semaphores. Data moves between devices by JAX's collectives and lax.ppermute only.
A program may use at most 64 MiB of HBM per device.

v0:
```python
import jax
import jax.numpy as jnp
from jax import lax
from jax.sharding import Mesh
from jax.sharding import PartitionSpec as P

RA = ("ra_0", "ra_1")


EPS = 1e-06
RESIDUAL = 0.5


def shifted(value, axis, steps):
    count = lax.axis_size(axis)
    initial, last = (max(0, -steps), min(count, count - steps))
    return lax.ppermute(value, axis, [(source, source + steps) for source in range(initial, last)])


def sent_together(arrays, axis, dim, along):
    ends, at = ([], 0)
    for a in arrays[:-1]:
        at += a.shape[along]
        ends.append(at)
    both = jnp.concatenate(arrays, axis=along)
    return tuple(jnp.split(lax.all_gather(both, axis, axis=dim, tiled=True), ends, axis=along))


def gather_axes(value, axes, dim):
    whole = value
    for number in range(len(axes) - 1, -1, -1):
        whole = lax.all_gather(whole, axes[number], axis=dim, tiled=True)
    return whole


def padded_to(lines, length):
    spare = -len(lines) % length
    return jnp.pad(lines, [(0, spare)] + [(0, 0)] * (lines.ndim - 1))


def total_of(value, axis):
    lines = value.reshape(-1, *value.shape[1:][-1:])
    own = lax.psum_scatter(
        padded_to(lines, lax.axis_size(axis)), axis, scatter_dimension=0, tiled=True
    )
    whole = lax.all_gather(own, axis).reshape(-1, *lines.shape[1:])
    return lax.slice_in_dim(whole, 0, len(lines)).reshape(value.shape)


def valid_taps(values, taps):
    width = taps.shape[0]
    length = values.shape[0] - width + 1
    total = taps[0][None, :] * values[0:length]
    for k in range(1, width):
        total = total + taps[k][None, :] * values[k : k + length]
    return total


def per_device(
    tokens,
    norm_gain,
    up_weight,
    gate_weight,
    up_scale,
    gate_scale,
    up_taps,
    gate_taps,
    down_weight,
    down_scale,
):
    state = lax.all_to_all(tokens, RA, split_axis=1, concat_axis=0, tiled=True).T
    edge = up_taps.shape[1] - 1
    for layer in range(up_weight.shape[0]):
        before = shifted(state[state.shape[0] - edge :], RA, 1)
        rows = jnp.concatenate([before, state], axis=0)
        rows_f = rows.astype(jnp.float32)
        inverse = lax.rsqrt(jnp.mean(rows_f * rows_f, axis=1, keepdims=True) + EPS)
        scaled = (rows_f * norm_gain[layer][None, :]).astype(jnp.bfloat16)
        pieces = sent_together(
            (up_weight[layer].astype(jnp.bfloat16), gate_weight[layer].astype(jnp.bfloat16)),
            RA,
            0,
            1,
        )
        up_raw = jnp.dot(scaled, pieces[0], preferred_element_type=jnp.float32)
        gate_raw = jnp.dot(scaled, pieces[1], preferred_element_type=jnp.float32)
        up_pre = up_raw * inverse * up_scale[layer][None, :]
        gate_pre = gate_raw * inverse * gate_scale[layer][None, :]
        conv_up = valid_taps(up_pre, up_taps[layer])
        conv_gate = valid_taps(gate_pre, gate_taps[layer])
        hidden = (jax.nn.silu(conv_gate) * conv_up).astype(jnp.bfloat16)
        down_part = lax.dot_general(
            hidden,
            gather_axes(down_weight[layer].astype(jnp.bfloat16), RA, 0),
            (((1,), (1,)), ((), ())),
            preferred_element_type=jnp.float32,
        )
        down = total_of(down_part.astype(jnp.bfloat16), "cb").astype(jnp.float32)
        state = (down * down_scale[layer][None, :] + RESIDUAL * state.astype(jnp.float32)).astype(
            jnp.bfloat16
        )
    return lax.all_to_all(state.T, RA, split_axis=0, concat_axis=1, tiled=True)


def solution(mesh):
    torus = Mesh(mesh.devices.reshape(8, 4, mesh.shape["cb"]), ("ra_0", "ra_1", "cb"))
    placed = (
        P(RA, None),
        P(),
        P(None, RA, "cb"),
        P(None, RA, "cb"),
        P(None, "cb"),
        P(None, "cb"),
        P(None, None, "cb"),
        P(None, None, "cb"),
        P(None, RA, "cb"),
        P(),
    )
    return jax.shard_map(
        per_device, mesh=torus, in_specs=placed, out_specs=P(RA, None), check_vma=False
    )
```

profile of v0, /device:TPU:1, one launch (start us, length us, event | category | flops | bytes accessed | tf_op | source)
XLA Modules:
  0.0 511.3 jit_solution(13660260227973896724)
XLA Ops:
  6.5 1.2 convert.14
  7.7 1.0 convert.15
  9.5 1.6 copy.26
  11.1 12.2 %all-to-all-start = ((bf16[64,32,512]{2,0,1:T(8,128)(2,1)}), bf16[64,32,512]{2,0,1:T(8,128)(2,1)S(1)}, u32[]{:S(2)}, u32[]{:S(2)}) async-start(bf16[64,32,512]{2,0,1:T(8,128)(2,1)} %bitcast.42), calls=%async_computation | async-start | bytes 4194304 | tf_op jit(solution)/shard_map/all_to_all | solution.py:71
  23.4 16.6 %all-gather = bf16[1,256,768]{2,1,0:T(8,128)(2,1)} all-gather(bf16[1,64,768]{2,1,0:T(8,128)(2,1)S(1)} %get-tuple-element.26), channel_id=2, replica_groups=mesh['ra_0'=8,'ra_1'=4,'cb'=8] {'ra_1'}, dimensions={1}, use_global_device_ids=true | all-gather | bytes 491520 | tf_op jit(solution)/shard_map/all_gather | solution.py:32
  40.3 38.9 %all-to-all-done = bf16[64,32,512]{2,0,1:T(8,128)(2,1)S(1)} async-done(((bf16[64,32,512]{2,0,1:T(8,128)(2,1)}), bf16[64,32,512]{2,0,1:T(8,128)(2,1)S(1)}, u32[]{:S(2)}, u32[]{:S(2)}) %all-to-all-start) | async-done | bytes 2097184 | tf_op jit(solution)/shard_map/all_to_all | solution.py:71
  79.2 1.3 copy-done.2
  80.5 3.0 copy.20
  83.5 4.0 collective-permute-start
  88.4 0.8 fusion.1
  89.2 23.7 %all-gather.13.cloned.1.call-done = bf16[2048,1536]{1,0:T(8,128)(2,1)} async-done(((bf16[64,1536]{1,0:T(8,128)(2,1)}), bf16[2048,1536]{1,0:T(8,128)(2,1)}) %all-gather.13.cloned.1.call-update) | async-done | bytes 6291472 | tf_op jit(solution)/shard_map/all_gather | solution.py:26
  112.9 5.2 %multiply_multiply_fusion.3 = f32[514,768]{1,0:T(8,128)} fusion(bf16[2048,1536]{1,0:T(8,128)(2,1)} %all-gather.13.cloned.1.call-done, f32[2048]{0:T(1024)S(1)} %bitcast.50, f32[768]{0:T(1024)S(1)} %get-tuple-element.18, f32[514]{0:T(1024)S(1)} %add_rsqrt_fusion.1, bf16[512,2048]{1,0:T(8,128)(2,1)S(1)} %bitcast.39, bf16[2,2048]{1,0:T(2,128)(2,1)S(1)} %collective-permute-done), kind=kOutput, calls=%fused_computation.35 | convolution fusion | flops 1624009728 | bytes 6843400 | tf_op jit(solution)/shard_map/dot_general | solution.py:86
  118.1 3.1 multiply_multiply_fusion.2
  121.2 35.7 %all-gather.17.cloned.1.call-done = bf16[1,2048,768]{2,1,0:T(8,128)(2,1)} async-done(((bf16[1,256,768]{2,1,0:T(8,128)(2,1)}), bf16[1,2048,768]{2,1,0:T(8,128)(2,1)}) %all-gather.17.cloned.1.call-update) | async-done | bytes 3145744 | tf_op jit(solution)/shard_map/all_gather | solution.py:32
  156.9 8.9 %fusion.20 = bf16[512,2048]{1,0:T(8,128)(2,1)} fusion(bf16[1,2048,768]{2,1,0:T(8,128)(2,1)} %all-gather.17.cloned.1.call-done, f32[514,768]{1,0:T(8,128)} %multiply_multiply_fusion.2, f32[514,768]{1,0:T(8,128)} %multiply_multiply_fusion.3, f32[768]{0:T(1024)S(1)} %get-tuple-element.12, f32[768]{0:T(1024)S(1)} %get-tuple-element.13, ...), kind=kOutput, calls=%fused_computation.26 | convolution fusion | flops 1617952768 | bytes 14698496 | tf_op jit(solution)/shard_map/dot_general | solution.py:92
  165.8 33.2 %reduce-scatter.3.cloned.1.call-done = bf16[64,2048]{1,0:T(8,128)(2,1)} async-done(((bf16[512,2048]{1,0:T(8,128)(2,1)}), bf16[64,2048]{1,0:T(8,128)(2,1)}) %reduce-scatter.3.cloned.1.call-update) | async-done | bytes 262160 | tf_op jit(solution)/shard_map/reduce_scatter | solution.py:43
  199.9 10.5 %all-gather.3 = bf16[1,256,768]{2,1,0:T(8,128)(2,1)} all-gather(bf16[1,64,768]{2,1,0:T(8,128)(2,1)S(1)} %get-tuple-element.25), channel_id=5, replica_groups=mesh['ra_0'=8,'ra_1'=4,'cb'=8] {'ra_1'}, dimensions={1}, use_global_device_ids=true | all-gather | bytes 491520 | tf_op jit(solution)/shard_map/all_gather | solution.py:32
  210.5 19.8 %all-gather.19.cloned.1.call-done = bf16[512,2048]{1,0:T(8,128)(2,1)} async-done(((bf16[64,2048]{1,0:T(8,128)(2,1)}), bf16[512,2048]{1,0:T(8,128)(2,1)}) %all-gather.19.cloned.1.call-update) | async-done | bytes 2097168 | tf_op jit(solution)/shard_map/all_gather | solution.py:46
  230.3 2.5 fusion.7
  232.8 3.3 collective-permute-start.1
  236.7 0.8 fusion.3
  237.6 82.5 %all-gather.15.cloned.1.call-done = bf16[2048,1536]{1,0:T(8,128)(2,1)} async-done(((bf16[64,1536]{1,0:T(8,128)(2,1)}), bf16[2048,1536]{1,0:T(8,128)(2,1)}) %all-gather.15.cloned.1.call-update) | async-done | bytes 6291472 | tf_op jit(solution)/shard_map/all_gather | solution.py:26
  320.1 5.8 %multiply_multiply_fusion.1 = f32[514,768]{1,0:T(8,128)} fusion(bf16[2048,1536]{1,0:T(8,128)(2,1)} %all-gather.15.cloned.1.call-done, f32[2048]{0:T(1024)S(1)} %bitcast.48, f32[768]{0:T(1024)S(1)} %get-tuple-element.17, f32[514]{0:T(1024)S(1)} %add_rsqrt_fusion, bf16[512,2048]{1,0:T(8,128)(2,1)} %copy-done, bf16[2,2048]{1,0:T(2,128)(2,1)S(1)} %collective-permute-done.1), kind=kOutput, calls=%fused_computation.33 | convolution fusion | flops 1624009728 | bytes 6843400 | tf_op jit(solution)/shard_map/dot_general | solution.py:86
  325.9 3.1 multiply_multiply_fusion
  329.0 35.0 %all-gather.21.cloned.1.call-done = bf16[1,2048,768]{2,1,0:T(8,128)(2,1)} async-done(((bf16[1,256,768]{2,1,0:T(8,128)(2,1)}), bf16[1,2048,768]{2,1,0:T(8,128)(2,1)}) %all-gather.21.cloned.1.call-update) | async-done | bytes 3145744 | tf_op jit(solution)/shard_map/all_gather | solution.py:32
  364.0 8.9 %fusion.23 = bf16[512,2048]{1,0:T(8,128)(2,1)} fusion(bf16[1,2048,768]{2,1,0:T(8,128)(2,1)} %all-gather.21.cloned.1.call-done, f32[514,768]{1,0:T(8,128)} %multiply_multiply_fusion, f32[514,768]{1,0:T(8,128)} %multiply_multiply_fusion.1, f32[768]{0:T(1024)S(1)} %get-tuple-element.15, f32[768]{0:T(1024)S(1)} %get-tuple-element.16, ...), kind=kOutput, calls=%fused_computation.27 | convolution fusion | flops 1617952768 | bytes 14698496 | tf_op jit(solution)/shard_map/dot_general | solution.py:92
  373.0 33.2 %reduce-scatter.5.cloned.1.call-done = bf16[64,2048]{1,0:T(8,128)(2,1)} async-done(((bf16[512,2048]{1,0:T(8,128)(2,1)}), bf16[64,2048]{1,0:T(8,128)(2,1)}) %reduce-scatter.5.cloned.1.call-update) | async-done | bytes 262160 | tf_op jit(solution)/shard_map/reduce_scatter | solution.py:43
  406.2 31.4 %all-gather.23.cloned.1.call-done = bf16[512,2048]{1,0:T(8,128)(2,1)} async-done(((bf16[64,2048]{1,0:T(8,128)(2,1)}), bf16[512,2048]{1,0:T(8,128)(2,1)}) %all-gather.23.cloned.1.call-update) | async-done | bytes 2097168 | tf_op jit(solution)/shard_map/all_gather | solution.py:46
  437.6 3.8 fusion.26
  441.4 2.9 copy.21
  444.3 58.7 %all_to_all.38 = bf16[32,64,512]{2,1,0:T(8,128)(2,1)S(1)} all-to-all(bf16[32,64,512]{2,1,0:T(8,128)(2,1)S(1)} %bitcast.43), channel_id=1, replica_groups=mesh['ra_0'=8,'ra_1'=4,'cb'=8] {'ra_0','ra_1'}, dimensions={0} | all-to-all | bytes 4194304 | tf_op jit(solution)/shard_map/all_to_all | solution.py:102
  503.0 1.5 copy.24
  (57 shorter events, 3.6 us)
Async XLA Ops:
  6.5 3.0 copy-start.3
  6.5 106.4 %all-gather.13.cloned.1.call-start = ((), (), s32[]{:S(2)}) async-start(), calls=%async_computation.4 | async-start | bytes 6488064 | tf_op jit(solution)/shard_map/all_gather | solution.py:26
  11.1 12.2 %copy-start.4 = (f32[2,64,768]{2,1,0:T(8,128)S(1)}, f32[2,64,768]{2,1,0:T(8,128)}, u32[]{:S(2)}) copy-start(f32[2,64,768]{2,1,0:T(8,128)} %param.18) | copy-start | bytes 1179652
  11.1 29.0 %copy-start.9 = (f32[2,768]{1,0:T(2,128)S(1)}, f32[2,768]{1,0:T(2,128)}, u32[]{:S(2)}) copy-start(f32[2,768]{1,0:T(2,128)} %param.15) | copy-start | bytes 18436
  11.1 29.0 %copy-start.5 = (f32[2,3,768]{2,0,1:T(2,128)S(1)}, f32[2,3,768]{2,0,1:T(2,128)}, u32[]{:S(2)}) copy-start(f32[2,3,768]{2,0,1:T(2,128)} %param.16) | copy-start | bytes 55300
  11.1 29.0 %copy-start.6 = (f32[2,3,768]{2,0,1:T(2,128)S(1)}, f32[2,3,768]{2,0,1:T(2,128)}, u32[]{:S(2)}) copy-start(f32[2,3,768]{2,0,1:T(2,128)} %param.17) | copy-start | bytes 55300
  11.1 29.1 %copy-start.7 = (f32[2,2048]{1,0:T(2,128)S(1)}, f32[2,2048]{1,0:T(2,128)}, u32[]{:S(2)}) copy-start(f32[2,2048]{1,0:T(2,128)} %param.11) | copy-start | bytes 49156
  11.1 68.0 %all-to-all-start = ((bf16[64,32,512]{2,0,1:T(8,128)(2,1)}), bf16[64,32,512]{2,0,1:T(8,128)(2,1)S(1)}, u32[]{:S(2)}, u32[]{:S(2)}) async-start(bf16[64,32,512]{2,0,1:T(8,128)(2,1)} %bitcast.42), calls=%async_computation | async-start | bytes 4194304 | tf_op jit(solution)/shard_map/all_to_all | solution.py:71
  23.3 133.6 %all-gather.17.cloned.1.call-start = ((), (), s32[]{:S(2)}) async-start(), calls=%async_computation.8 | async-start | bytes 3538944 | tf_op jit(solution)/shard_map/all_gather | solution.py:32
  40.0 159.0 %reduce-scatter.3.cloned.1.call-start = ((), (), s32[]{:S(2)}) async-start(), calls=%async_computation.5 | async-start | bytes 2359296 | tf_op jit(solution)/shard_map/reduce_scatter | solution.py:43
  79.2 1.3 copy-start.2
  80.5 7.0 %copy-start.10 = (f32[2,768]{1,0:T(2,128)S(1)}, f32[2,768]{1,0:T(2,128)}, u32[]{:S(2)}) copy-start(f32[2,768]{1,0:T(2,128)} %param.14) | copy-start | bytes 18436
  83.5 4.9 collective-permute-start
  112.9 5.2 %copy-start.11 = (bf16[2048,1536]{1,0:T(8,128)(2,1)S(1)}, bf16[2048,1536]{1,0:T(8,128)(2,1)}, u32[]{:S(2)}) copy-start(bf16[2048,1536]{1,0:T(8,128)(2,1)} %all-gather.13.cloned.1.call-done) | copy-start | bytes 18874372
  165.8 44.7 %copy-start.8 = (f32[2,2048]{1,0:T(2,128)S(1)}, f32[2,2048]{1,0:T(2,128)}, u32[]{:S(2)}) copy-start(f32[2,2048]{1,0:T(2,128)} %param.19) | copy-start | bytes 49156
  165.8 64.5 %all-gather.19.cloned.1.call-start = ((), (), s32[]{:S(2)}) async-start(), calls=%async_computation.9 | async-start | bytes 2359296 | tf_op jit(solution)/shard_map/all_gather | solution.py:46
  199.1 121.0 %all-gather.15.cloned.1.call-start = ((), (), s32[]{:S(2)}) async-start(), calls=%async_computation.6 | async-start | bytes 6488064 | tf_op jit(solution)/shard_map/all_gather | solution.py:26
  199.9 164.2 %all-gather.21.cloned.1.call-start = ((), (), s32[]{:S(2)}) async-start(), calls=%async_computation.10 | async-start | bytes 3538944 | tf_op jit(solution)/shard_map/all_gather | solution.py:32
  210.4 195.8 %reduce-scatter.5.cloned.1.call-start = ((), (), s32[]{:S(2)}) async-start(), calls=%async_computation.7 | async-start | bytes 2359296 | tf_op jit(solution)/shard_map/reduce_scatter | solution.py:43
  232.8 3.9 copy-start
  232.8 3.9 collective-permute-start.1
  320.1 5.8 %copy-start.1 = (bf16[512,2048]{1,0:T(8,128)(2,1)S(1)}, bf16[512,2048]{1,0:T(8,128)(2,1)}, u32[]{:S(2)}) copy-start(bf16[512,2048]{1,0:T(8,128)(2,1)} %copy-done) | copy-start | bytes 6291460
  320.1 5.8 %copy-start.12 = (bf16[2048,1536]{1,0:T(8,128)(2,1)S(1)}, bf16[2048,1536]{1,0:T(8,128)(2,1)}, u32[]{:S(2)}) copy-start(bf16[2048,1536]{1,0:T(8,128)(2,1)} %all-gather.15.cloned.1.call-done) | copy-start | bytes 18874372
  372.9 64.7 %all-gather.23.cloned.1.call-start = ((), (), s32[]{:S(2)}) async-start(), calls=%async_computation.11 | async-start | bytes 2359296 | tf_op jit(solution)/shard_map/all_gather | solution.py:46
Sparse Core Ops, SparseCore 0:
  9.9 102.9 all-gather.12
  114.7 42.0 all-gather.16
  165.9 33.1 reduce-scatter.2
  200.8 29.4 all-gather.18
  232.7 87.2 all-gather.14
  321.7 42.2 all-gather.20
  373.1 33.1 reduce-scatter.4
  408.1 29.4 all-gather.22
where the time goes:
time: 513 us; the launch traced here: 511 us
  waiting for transfers between devices  335 us (65%)
  blocking collectives  85.8 us (17%)
  matrix products  34.9 us (7%)
  starting transfers between devices  19.8 us (4%)
  between operations  13.7 us (3%)
  other arithmetic  11.6 us (2%)
  local copies, waits for them, and re-layouts  10.5 us (2%)
    all_gather x2, waiting for transfers between devices, sent_together(): lax.all_gather(both, axis, axis=dim, tiled=True)  106 us
    all_gather x2, waiting for transfers between devices, gather_axes(): whole = lax.all_gather(whole, axes[number], axis=dim, tiled=True)  70.7 us
    reduce_scatter x2, waiting for transfers between devices, total_of(): lax.psum_scatter(padded_to(lines, lax.axis_size(axis)), axis, scatter_dim...  66.4 us
    all_to_all x1, blocking collectives, per_device(): return lax.all_to_all(state.T, RA, split_axis=0, concat_axis=1, tiled=True)  58.7 us
    all_gather x2, waiting for transfers between devices, total_of(): whole = lax.all_gather(own, axis).reshape(-1, *lines.shape[1:])  51.2 us
    all_to_all x1, waiting for transfers between devices, per_device(): lax.all_to_all(tokens, RA, split_axis=1, concat_axis=0, tiled=True)  38.9 us
    all_gather x2, blocking collectives, gather_axes(): whole = lax.all_gather(whole, axes[number], axis=dim, tiled=True)  27.1 us
    dot_general x2, matrix products, per_device(): lax.dot_general(hidden, gather_axes(down_weight[layer].astype(jnp.bfloat1...  17.8 us
  transfers between devices with their start and end apart: 11, of which 11 were waited for; matrix products, arithmetic and copies ran while one was open for 5% of the time, Pallas kernels for 0%

commit v1 on v0

v1 whole, which is shorter than its diff:
```python
import jax
import jax.numpy as jnp
from jax import lax
from jax.sharding import Mesh
from jax.sharding import PartitionSpec as P

RA = ("z", "y")
CB = ("x", "c")
EPS = 1e-06
RESIDUAL = 0.5
BF = jnp.bfloat16
F32 = jnp.float32


def turned(value, axis, steps):
    count = lax.axis_size(axis)
    return lax.ppermute(value, axis, [(s, (s + steps) % count) for s in range(count)])


def shifted(value, axis, steps):
    count = lax.axis_size(axis)
    initial, last = (max(0, -steps), min(count, count - steps))
    return lax.ppermute(value, axis, [(s, s + steps) for s in range(initial, last)])


def at(blocks, index):
    return lax.dynamic_index_in_dim(blocks, index, 0, keepdims=False)


def gather_cb(own):
    half = own.shape[0] // 2
    x = lax.axis_index("x")
    c = lax.axis_index("c")
    left = turned(own, "x", 1)
    right = turned(own, "x", -1)
    far_low = turned(left[:half], "x", 1)
    far_high = turned(right[half:], "x", -1)
    far = jnp.concatenate([far_low, far_high], axis=0)
    whole = jnp.zeros((4, *own.shape), own.dtype)
    for steps, block in ((0, own), (3, left), (1, right), (2, far)):
        whole = lax.dynamic_update_index_in_dim(whole, block, (x + steps) % 4, 0)
    other = turned(whole, "c", 1)
    first = jnp.where(c == 0, whole, other)
    second = jnp.where(c == 0, other, whole)
    return jnp.stack([first, second], axis=1)


def scatter_cb(parts):
    x = lax.axis_index("x")
    c = lax.axis_index("c")
    mine = jnp.where(c == 0, parts[:, 0], parts[:, 1])
    sent = jnp.where(c == 0, parts[:, 1], parts[:, 0])
    pair = (mine.astype(F32) + turned(sent, "c", 1).astype(F32)).astype(BF)
    half = pair.shape[1] // 2
    far = at(pair, (x + 2) % 4)
    from_left = turned(far[:half], "x", 1)
    from_right = turned(far[half:], "x", -1)
    to_right = at(pair, (x + 1) % 4)
    to_left = at(pair, (x + 3) % 4)
    low = (to_right[:half].astype(F32) + from_left.astype(F32)).astype(BF)
    high = (to_left[half:].astype(F32) + from_right.astype(F32)).astype(BF)
    a = turned(jnp.concatenate([low, to_right[half:]], axis=0), "x", 1)
    b = turned(jnp.concatenate([to_left[:half], high], axis=0), "x", -1)
    return at(pair, x).astype(F32) + a.astype(F32) + b.astype(F32)


def valid_taps(values, taps):
    width = taps.shape[0]
    length = values.shape[0] - width + 1
    total = taps[0][None, :] * values[0:length]
    for k in range(1, width):
        total = total + taps[k][None, :] * values[k : k + length]
    return total


def per_device(
    tokens,
    norm_gain,
    up_weight,
    gate_weight,
    up_scale,
    gate_scale,
    up_taps,
    gate_taps,
    down_weight,
    down_scale,
):
    layers = up_weight.shape[0]
    ra = lax.axis_size("z") * lax.axis_size("y")
    cb = lax.axis_index("x") * 2 + lax.axis_index("c")
    rows, hid = up_weight.shape[1:]
    width = rows * ra
    part = rows // 8
    span = tokens.shape[1] // ra

    shards = [
        jnp.concatenate([w[l].astype(BF) for w in (up_weight, gate_weight, down_weight)], axis=1)
        for l in range(layers)
    ]
    weights = [lax.all_gather(s, RA, axis=0, tiled=True) for s in shards]

    own = lax.dynamic_slice_in_dim(tokens, cb * part, part, 0)
    own = own.reshape(part, ra, span).transpose(1, 0, 2)
    own = lax.all_to_all(own, RA, split_axis=0, concat_axis=0, tiled=True)
    every = gather_cb(own)
    state = every.reshape(8, ra, part, span).transpose(3, 1, 0, 2).reshape(span, width)

    edge = up_taps.shape[1] - 1
    for l in range(layers):
        before = shifted(state[span - edge :], RA, 1)
        rows_all = jnp.concatenate([before, state], axis=0)
        rows_f = rows_all.astype(F32)
        inverse = lax.rsqrt(jnp.mean(rows_f * rows_f, axis=1, keepdims=True) + EPS)
        scaled = (rows_f * norm_gain[l][None, :]).astype(BF)
        w = weights[l]
        up_raw = jnp.dot(scaled, w[:, :hid], preferred_element_type=F32)
        gate_raw = jnp.dot(scaled, w[:, hid : 2 * hid], preferred_element_type=F32)
        conv_up = valid_taps(up_raw * inverse * up_scale[l][None, :], up_taps[l])
        conv_gate = valid_taps(gate_raw * inverse * gate_scale[l][None, :], gate_taps[l])
        hidden = (jax.nn.silu(conv_gate) * conv_up).astype(BF)
        down_w = w[:, 2 * hid :]
        if l + 1 < layers:
            down = lax.dot_general(
                hidden, down_w, (((1,), (1,)), ((), ())), preferred_element_type=F32
            ).astype(BF)
            piece = scatter_cb(down.reshape(4, 2, span // 8, width))
            held = lax.dynamic_slice_in_dim(state, cb * (span // 8), span // 8, 0)
            piece = (piece * down_scale[l][None, :] + RESIDUAL * held.astype(F32)).astype(BF)
            state = gather_cb(piece).reshape(span, width)
        else:
            down = lax.dot_general(
                down_w, hidden, (((1,), (1,)), ((), ())), preferred_element_type=F32
            ).astype(BF)
            down = down.reshape(ra, 4, 2, part, span).transpose(1, 2, 0, 3, 4)
            piece = scatter_cb(down)
            held = lax.dynamic_index_in_dim(
                state.reshape(span, ra, 8, part), cb, 2, keepdims=False
            ).transpose(1, 2, 0)
            scale = lax.dynamic_index_in_dim(
                down_scale[l].reshape(ra, 8, part), cb, 1, keepdims=False
            )
            piece = (piece * scale[:, :, None] + RESIDUAL * held.astype(F32)).astype(BF)
    piece = lax.all_to_all(piece, RA, split_axis=0, concat_axis=0, tiled=True)
    piece = piece.transpose(1, 0, 2).reshape(part, ra * span)
    return gather_cb(piece).reshape(rows, ra * span)


def solution(mesh):
    torus = Mesh(mesh.devices.reshape(8, 4, 4, 2), ("z", "y", "x", "c"))
    placed = (
        P(RA, None),
        P(),
        P(None, RA, CB),
        P(None, RA, CB),
        P(None, CB),
        P(None, CB),
        P(None, None, CB),
        P(None, None, CB),
        P(None, RA, CB),
        P(),
    )
    return jax.shard_map(
        per_device, mesh=torus, in_specs=placed, out_specs=P(RA, None), check_vma=False
    )
```

time: 513 us -> 321 us (0.63)
  waiting for transfers between devices: 335 us -> 126 us
  blocking collectives: 85.8 us -> 43.3 us
  starting transfers between devices: 19.8 us -> 52.4 us
  local copies, waits for them, and re-layouts: 10.5 us -> 39.1 us
  matrix products: 34.9 us -> 19.4 us
  other arithmetic: 11.6 us -> 21.6 us
    all_gather x6 -> x2, waiting for transfers between devices: 228 us -> 54.1 us  [per_device(): weights = [lax.all_gather(s, RA, axis=0, tiled=True) for s in shards]]
    ppermute x2 -> x27, waiting for transfers between devices: 1.43 us -> 71.5 us  [the longest x25 70.9 us: turned(): lax.ppermute(value, axis, [(s, (s + steps) % count) for s in range(count)])]
    reduce_scatter x2 -> x0, waiting for transfers between devices: 66.4 us -> none  [total_of(): lax.psum_scatter(padded_to(lines, lax.axis_size(axis)), axis, scatter_dim...]
    ppermute x2 -> x27, starting transfers between devices: 7.3 us -> 52.3 us  [the longest x25 47.4 us: turned(): lax.ppermute(value, axis, [(s, (s + steps) % count) for s in range(count)])]
    all_to_all x1 -> x0, waiting for transfers between devices: 38.9 us -> none  [per_device(): lax.all_to_all(tokens, RA, split_axis=1, concat_axis=0, tiled=True)]
    all_gather x2 -> x0, blocking collectives: 27.1 us -> none  [gather_axes(): whole = lax.all_gather(whole, axes[number], axis=dim, tiled=True)]
    another operation x0 -> x4, local copies, waits for them, and re-layouts: none -> 17.2 us  [the longest x1 9.35 us: per_device(): state.reshape(span, ra, 8, part)]
    dot_general x6, matrix products: 34.9 us -> 19.4 us  [the longest x2 9.18 us: per_device(): gate_raw = jnp.dot(scaled, w[:, hid:2 * hid], preferred_element_type=F32)]
  transfers between devices with their start and end apart: 11 -> 29, of which waited for: 11 -> 17; matrix products, arithmetic and copies ran while one was open for 5% -> 18% of each run, Pallas kernels for 0% -> 0%
where the time goes in v1:
time: 321 us; the launch traced here: 316 us
  waiting for transfers between devices  126 us (39%)
  starting transfers between devices  52.4 us (16%)
  blocking collectives  43.3 us (13%)
  local copies, waits for them, and re-layouts  39.1 us (12%)
  other arithmetic  21.6 us (7%)
  matrix products  19.4 us (6%)
  between operations  14.5 us (5%)
    ppermute x25, waiting for transfers between devices, turned(): lax.ppermute(value, axis, [(s, (s + steps) % count) for s in range(count)])  70.9 us
    all_gather x2, waiting for transfers between devices, per_device(): weights = [lax.all_gather(s, RA, axis=0, tiled=True) for s in shards]  54.1 us
    ppermute x25, starting transfers between devices, turned(): lax.ppermute(value, axis, [(s, (s + steps) % count) for s in range(count)])  47.4 us
    all_to_all x1, blocking collectives, per_device(): own = lax.all_to_all(own, RA, split_axis=0, concat_axis=0, tiled=True)  23.3 us
    all_to_all x1, blocking collectives, per_device(): piece = lax.all_to_all(piece, RA, split_axis=0, concat_axis=0, tiled=True)  20 us
    another operation x1, local copies, waits for them, and re-layouts, per_device(): state.reshape(span, ra, 8, part)  9.35 us
    dot_general x2, matrix products, per_device(): gate_raw = jnp.dot(scaled, w[:, hid:2 * hid], preferred_element_type=F32)  9.18 us
    another operation x2, local copies, waits for them, and re-layouts, gather_cb(): return jnp.stack([first, second], axis=1)  7.73 us
  transfers between devices with their start and end apart: 29, of which 17 were waited for; matrix products, arithmetic and copies ran while one was open for 18% of the time, Pallas kernels for 0%

profile of v1, /device:TPU:1, one launch (start us, length us, event | category | flops | bytes accessed | tf_op | source)
XLA Modules:
  0.0 315.9 jit_solution(3003010898439355616)
XLA Ops:
  11.5 23.3 %all_to_all.10 = bf16[32,8,512]{2,1,0:T(8,128)(2,1)S(1)} all-to-all(bf16[32,8,512]{2,1,0:T(8,128)(2,1)S(1)} %bitcast.156), channel_id=1, replica_groups=mesh['z'=8,'y'=4,'x'=4,'c'=2] {'z','y'}, dimensions={0} | all-to-all | bytes 524288 | tf_op jit(solution)/shard_map/all_to_all | solution.py:104
  37.5 4.0 %collective-permute-done = bf16[32,8,512]{2,1,0:T(8,128)(2,1)S(1)} collective-permute-done((bf16[32,8,512]{2,1,0:T(8,128)(2,1)S(1)}, bf16[32,8,512]{2,1,0:T(8,128)(2,1)S(1)}, u32[]{:S(2)}, u32[]{:S(2)}) %collective-permute-start) | collective-permute-done | bytes 262176 | tf_op jit(solution)/shard_map/ppermute | solution.py:17
  41.7 2.7 collective-permute-start.3
  46.7 4.6 %collective-permute-start.4 = (bf16[4,32,8,512]{3,2,1,0:T(8,128)(2,1)S(1)}, bf16[4,32,8,512]{3,2,1,0:T(8,128)(2,1)S(1)}, u32[]{:S(2)}, u32[]{:S(2)}) collective-permute-start(bf16[4,32,8,512]{3,2,1,0:T(8,128)(2,1)S(1)} %fusion.75), channel_id=1, source_target_pairs={{0,1},{1,0},{2,3},{3,2},{4,5},{5,4},{6,7},{7,6},{8,9},{9,8},{10,11... | collective-permute-start | bytes 3145736 | tf_op jit(solution)/shard_map/ppermute | solution.py:17
  56.3 2.9 collective-permute-start.5
  63.1 54.1 %all-gather.5.cloned.1.call-done = bf16[2048,2304]{1,0:T(8,128)(2,1)} async-done(((bf16[64,2304]{1,0:T(8,128)(2,1)}), bf16[2048,2304]{1,0:T(8,128)(2,1)}) %all-gather.5.cloned.1.call-update) | async-done | bytes 9437200 | tf_op jit(solution)/shard_map/all_gather | solution.py:100
  117.2 5.2 %multiply_multiply_fusion.3 = f32[514,768]{1,0:T(8,128)S(1)} fusion(bf16[2048,2304]{1,0:T(8,128)(2,1)} %all-gather.5.cloned.1.call-done, f32[768]{0:T(1024)S(1)} %get-tuple-element.18, f32[514]{0:T(1024)S(1)} %add_rsqrt_fusion.1, f32[2048]{0:T(1024)S(1)} %bitcast.163, bf16[512,2048]{0,1:T(8,128)(2,1)S(1)} %bitcast.144, bf16[2,2048]{0,1:T(8,128)(2,1)S(1)} %copy.55), kind=kOutput, calls=%fused_computation.36 | convolution fusion | flops 1624009728 | bytes 6843400 | tf_op jit(solution)/shard_map/dot_general | solution.py:117
  122.4 3.2 %multiply_multiply_fusion.2 = f32[514,768]{1,0:T(8,128)S(1)} fusion(bf16[2048,2304]{1,0:T(8,128)(2,1)S(1)} %copy-done.14, f32[768]{0:T(1024)S(1)} %get-tuple-element.19, f32[514]{0:T(1024)S(1)} %add_rsqrt_fusion.1, f32[2048]{0:T(1024)S(1)} %bitcast.164, bf16[512,2048]{0,1:T(8,128)(2,1)S(1)} %bitcast.145, bf16[2,2048]{0,1:T(8,128)(2,1)S(1)} %copy.55), kind=kOutput, calls=%fused_computation.35 | convolution fusion | flops 1624009728 | bytes 7362560 | tf_op jit(solution)/shard_map/dot_general | solution.py:116
  125.7 2.7 fusion.20
  136.8 3.2 %collective-permute-start.6 = (bf16[4,64,2048]{2,1,0:T(8,128)(2,1)S(1)}, bf16[4,64,2048]{2,1,0:T(8,128)(2,1)}, u32[]{:S(2)}, u32[]{:S(2)}) collective-permute-start(bf16[4,64,2048]{2,1,0:T(8,128)(2,1)S(1)} %copy.58), channel_id=1, source_target_pairs={{0,1},{1,0},{2,3},{3,2},{4,5},{5,4},{6,7},{7,6},{8,9},{9,8},{10,11... | collective-permute-start | bytes 3145736 | tf_op jit(solution)/shard_map/ppermute | solution.py:17
  140.1 2.4 collective-permute-done.6
  142.5 2.7 copy.59
  145.2 3.1 fusion.4
  151.5 12.3 %collective-permute-done.7 = bf16[32,2048]{0,1:T(8,128)(2,1)S(1)} collective-permute-done((bf16[32,2048]{0,1:T(8,128)(2,1)S(1)}, bf16[32,2048]{0,1:T(8,128)(2,1)S(1)}, u32[]{:S(2)}, u32[]{:S(2)}) %collective-permute-start.7) | collective-permute-done | bytes 131104 | tf_op jit(solution)/shard_map/ppermute | solution.py:17
  167.6 11.2 %collective-permute-done.8 = bf16[64,2048]{0,1:T(8,128)(2,1)S(1)} collective-permute-done((bf16[64,2048]{0,1:T(8,128)(2,1)S(1)}, bf16[64,2048]{0,1:T(8,128)(2,1)S(1)}, u32[]{:S(2)}, u32[]{:S(2)}) %collective-permute-start.8) | collective-permute-done | bytes 262176 | tf_op jit(solution)/shard_map/ppermute | solution.py:17
  180.5 2.8 collective-permute-start.12
  183.7 9.3 %collective-permute-done.12 = bf16[64,2048]{0,1:T(8,128)(2,1)S(1)} collective-permute-done((bf16[64,2048]{0,1:T(8,128)(2,1)S(1)}, bf16[64,2048]{0,1:T(8,128)(2,1)S(1)}, u32[]{:S(2)}, u32[]{:S(2)}) %collective-permute-start.12) | collective-permute-done | bytes 262176 | tf_op jit(solution)/shard_map/ppermute | solution.py:17
  194.0 3.5 %collective-permute-start.14 = (bf16[32,2048]{0,1:T(8,128)(2,1)}, bf16[32,2048]{0,1:T(8,128)(2,1)S(1)}, u32[]{:S(2)}, u32[]{:S(2)}) collective-permute-start(bf16[32,2048]{0,1:T(8,128)(2,1)} %slice.372), channel_id=1, source_target_pairs={{0,6},{2,0},{4,2},{6,4},{1,7},{3,1},{5,3},{7,5},{8,14},{10,8},{12,... | collective-permute-start | bytes 393224 | tf_op jit(solution)/shard_map/ppermute | solution.py:17
  199.9 6.9 %collective-permute-done.14 = bf16[32,2048]{0,1:T(8,128)(2,1)S(1)} collective-permute-done((bf16[32,2048]{0,1:T(8,128)(2,1)}, bf16[32,2048]{0,1:T(8,128)(2,1)S(1)}, u32[]{:S(2)}, u32[]{:S(2)}) %collective-permute-start.14) | collective-permute-done | bytes 131104 | tf_op jit(solution)/shard_map/ppermute | solution.py:17
  206.8 3.9 %collective-permute-done.13 = bf16[32,2048]{0,1:T(8,128)(2,1)S(1)} collective-permute-done((bf16[32,2048]{0,1:T(8,128)(2,1)}, bf16[32,2048]{0,1:T(8,128)(2,1)S(1)}, u32[]{:S(2)}, u32[]{:S(2)}) %collective-permute-start.13) | collective-permute-done | bytes 131104 | tf_op jit(solution)/shard_map/ppermute | solution.py:17
  211.3 3.4 %collective-permute-start.15 = (bf16[4,64,2048]{2,1,0:T(8,128)(2,1)S(1)}, bf16[4,64,2048]{2,1,0:T(8,128)(2,1)S(1)}, u32[]{:S(2)}, u32[]{:S(2)}) collective-permute-start(bf16[4,64,2048]{2,1,0:T(8,128)(2,1)S(1)} %constant_dynamic-update-slice_fusion.1), channel_id=1, source_target_pairs={{0,1},{1,0},{2,3},{3,2},{4,5},{5,4},{6,7},{7,6},{8,9},{9,8},{10,11... | collective-permute-start | bytes 3145736 | tf_op jit(solution)/shard_map/ppermute | solution.py:17
  220.8 4.0 %multiply_multiply_fusion.1 = f32[514,768]{1,0:T(8,128)S(1)} fusion(bf16[2048,2304]{1,0:T(8,128)(2,1)} %all-gather.3.cloned.1.call-done, f32[2048]{0:T(1024)S(1)} %bitcast.161, f32[768]{0:T(1024)S(1)} %get-tuple-element.17, f32[514]{0:T(1024)S(1)} %add_rsqrt_fusion, bf16[512,2048]{1,0:T(8,128)(2,1)S(1)} %bitcast.139, ...), kind=kOutput, calls=%fused_computation.34 | convolution fusion | flops 1624009728 | bytes 6843400 | tf_op jit(solution)/shard_map/dot_general | solution.py:117
  240.2 3.2 %collective-permute-done.18 = bf16[16,8,512]{2,1,0:T(8,128)(2,1)S(1)} collective-permute-done((bf16[16,8,512]{2,1,0:T(8,128)(2,1)S(1)}, bf16[16,8,512]{2,1,0:T(8,128)(2,1)S(1)}, u32[]{:S(2)}, u32[]{:S(2)}) %collective-permute-start.18) | collective-permute-done | bytes 131104 | tf_op jit(solution)/shard_map/ppermute | solution.py:17
  244.7 2.6 collective-permute-start.21
  247.4 7.5 %copy.66 = bf16[4,2,64,2048]{2,1,0,3:T(2,128)(2,1)} copy(bf16[4,2,64,2048]{3,2,1,0:T(8,128)(2,1)S(1)} %pad_maximum_fusion.3) | data formatting | bytes 4194304 | tf_op jit(solution)/shard_map/stack | solution.py:45
  254.9 9.3 %reshape_reshape.3 = bf16[512,32,8,8]{0,3,2,1:T(8,128)(2,1)S(1)} reshape(bf16[4,2,64,2048]{2,1,0,3:T(2,128)(2,1)} %copy.66) | data formatting | bytes 4194304 | tf_op jit(solution)/shard_map/reshape;reshape | solution.py:137
  265.5 20.0 %all_to_all.11 = bf16[32,8,512]{2,1,0:T(8,128)(2,1)S(1)} all-to-all(bf16[32,8,512]{2,1,0:T(8,128)(2,1)S(1)} %fusion.72), channel_id=1, replica_groups=mesh['z'=8,'y'=4,'x'=4,'c'=2] {'z','y'}, dimensions={0} | all-to-all | bytes 524288 | tf_op jit(solution)/shard_map/all_to_all | solution.py:143
  285.5 2.7 collective-permute-start.23
  288.3 3.6 %collective-permute-done.22 = bf16[8,16384]{1,0:T(8,128)(2,1)S(1)} collective-permute-done((bf16[8,16384]{1,0:T(8,128)(2,1)S(1)}, bf16[8,16384]{1,0:T(8,128)(2,1)S(1)}, u32[]{:S(2)}, u32[]{:S(2)}) %collective-permute-start.22) | collective-permute-done | bytes 262176 | tf_op jit(solution)/shard_map/ppermute | solution.py:17
  292.2 2.7 collective-permute-start.25
  295.0 2.6 collective-permute-done.24
  297.7 6.1 %collective-permute-start.26 = (bf16[4,8,16384]{2,1,0:T(8,128)(2,1)S(1)}, bf16[4,8,16384]{2,1,0:T(8,128)(2,1)S(1)}, u32[]{:S(2)}, u32[]{:S(2)}) collective-permute-start(bf16[4,8,16384]{2,1,0:T(8,128)(2,1)S(1)} %fusion.76), channel_id=1, source_target_pairs={{0,1},{1,0},{2,3},{3,2},{4,5},{5,4},{6,7},{7,6},{8,9},{9,8},{10,11... | collective-permute-start | bytes 3145736 | tf_op jit(solution)/shard_map/ppermute | solution.py:17
  (145 shorter events, 69.1 us)
Async XLA Ops:
  6.5 110.7 %all-gather.5.cloned.1.call-start = ((), (), s32[]{:S(2)}) async-start(), calls=%async_computation.3 | async-start | bytes 9732096 | tf_op jit(solution)/shard_map/all_gather | solution.py:100
  10.6 210.2 %all-gather.3.cloned.1.call-start = ((), (), s32[]{:S(2)}) async-start(), calls=%async_computation.2 | async-start | bytes 9732096 | tf_op jit(solution)/shard_map/all_gather | solution.py:100
  11.5 39.9 %copy-start.7 = (f32[2,3,768]{2,0,1:T(2,128)S(1)}, f32[2,3,768]{2,0,1:T(2,128)}, u32[]{:S(2)}) copy-start(f32[2,3,768]{2,0,1:T(2,128)} %param.16) | copy-start | bytes 55300
  11.5 40.0 %copy-start.9 = (f32[2,2048]{1,0:T(2,128)S(1)}, f32[2,2048]{1,0:T(2,128)}, u32[]{:S(2)}) copy-start(f32[2,2048]{1,0:T(2,128)} %param.11) | copy-start | bytes 49156
  34.8 6.8 %collective-permute-start = (bf16[32,8,512]{2,1,0:T(8,128)(2,1)S(1)}, bf16[32,8,512]{2,1,0:T(8,128)(2,1)S(1)}, u32[]{:S(2)}, u32[]{:S(2)}) collective-permute-start(bf16[32,8,512]{2,1,0:T(8,128)(2,1)S(1)} %all_to_all.10), channel_id=1, source_target_pairs={{0,2},{2,4},{4,6},{6,0},{1,3},{3,5},{5,7},{7,1},{8,10},{10,12},{12... | collective-permute-start | bytes 786440 | tf_op jit(solution)/shard_map/ppermute | solution.py:17
  36.0 5.7 %collective-permute-start.1 = (bf16[32,8,512]{2,1,0:T(8,128)(2,1)S(1)}, bf16[32,8,512]{2,1,0:T(8,128)(2,1)S(1)}, u32[]{:S(2)}, u32[]{:S(2)}) collective-permute-start(bf16[32,8,512]{2,1,0:T(8,128)(2,1)S(1)} %all_to_all.10), channel_id=1, source_target_pairs={{0,6},{2,0},{4,2},{6,4},{1,7},{3,1},{5,3},{7,5},{8,14},{10,8},{12,... | collective-permute-start | bytes 786440 | tf_op jit(solution)/shard_map/ppermute | solution.py:17
  41.6 5.1 %collective-permute-start.2 = (bf16[16,8,512]{2,1,0:T(8,128)(2,1)S(1)}, bf16[16,8,512]{2,1,0:T(8,128)(2,1)S(1)}, u32[]{:S(2)}, u32[]{:S(2)}) collective-permute-start(bf16[16,8,512]{2,1,0:T(8,128)(2,1)S(1)} %slice.354), channel_id=1, source_target_pairs={{0,2},{2,4},{4,6},{6,0},{1,3},{3,5},{5,7},{7,1},{8,10},{10,12},{12... | collective-permute-start | bytes 393224 | tf_op jit(solution)/shard_map/ppermute | solution.py:17
  41.7 5.0 %collective-permute-start.3 = (bf16[16,8,512]{2,1,0:T(8,128)(2,1)S(1)}, bf16[16,8,512]{2,1,0:T(8,128)(2,1)S(1)}, u32[]{:S(2)}, u32[]{:S(2)}) collective-permute-start(bf16[16,8,512]{2,1,0:T(8,128)(2,1)S(1)} %slice.355), channel_id=1, source_target_pairs={{0,6},{2,0},{4,2},{6,4},{1,7},{3,1},{5,3},{7,5},{8,14},{10,8},{12,... | collective-permute-start | bytes 393224 | tf_op jit(solution)/shard_map/ppermute | solution.py:17
  46.7 6.9 %collective-permute-start.4 = (bf16[4,32,8,512]{3,2,1,0:T(8,128)(2,1)S(1)}, bf16[4,32,8,512]{3,2,1,0:T(8,128)(2,1)S(1)}, u32[]{:S(2)}, u32[]{:S(2)}) collective-permute-start(bf16[4,32,8,512]{3,2,1,0:T(8,128)(2,1)S(1)} %fusion.75), channel_id=1, source_target_pairs={{0,1},{1,0},{2,3},{3,2},{4,5},{5,4},{6,7},{7,6},{8,9},{9,8},{10,11... | collective-permute-start | bytes 3145736 | tf_op jit(solution)/shard_map/ppermute | solution.py:17
  56.3 4.9 %collective-permute-start.5 = (bf16[2,2048]{1,0:T(2,128)(2,1)S(1)}, bf16[2,2048]{1,0:T(2,128)(2,1)S(1)}, u32[]{:S(2)}, u32[]{:S(2)}) collective-permute-start(bf16[2,2048]{1,0:T(2,128)(2,1)S(1)} %slice.282), channel_id=1, source_target_pairs={{0,8},{8,16},{16,24},{24,32},{32,40},{40,48},{48,56},{56,64},{64,7... | collective-permute-start | bytes 24584 | tf_op jit(solution)/shard_map/ppermute | solution.py:23
  61.2 61.3 %copy-start.4 = (bf16[512,32,8,8]{0,3,2,1:T(8,128)(2,1)}, bf16[512,32,8,8]{0,3,2,1:T(8,128)(2,1)S(1)}, u32[]{:S(2)}) copy-start(bf16[512,32,8,8]{0,3,2,1:T(8,128)(2,1)S(1)} %copy.54) | copy-start | bytes 6291460
  136.8 5.7 %collective-permute-start.6 = (bf16[4,64,2048]{2,1,0:T(8,128)(2,1)S(1)}, bf16[4,64,2048]{2,1,0:T(8,128)(2,1)}, u32[]{:S(2)}, u32[]{:S(2)}) collective-permute-start(bf16[4,64,2048]{2,1,0:T(8,128)(2,1)S(1)} %copy.58), channel_id=1, source_target_pairs={{0,1},{1,0},{2,3},{3,2},{4,5},{5,4},{6,7},{7,6},{8,9},{9,8},{10,11... | collective-permute-start | bytes 3145736 | tf_op jit(solution)/shard_map/ppermute | solution.py:17
  148.7 15.1 %collective-permute-start.7 = (bf16[32,2048]{0,1:T(8,128)(2,1)S(1)}, bf16[32,2048]{0,1:T(8,128)(2,1)S(1)}, u32[]{:S(2)}, u32[]{:S(2)}) collective-permute-start(bf16[32,2048]{0,1:T(8,128)(2,1)S(1)} %get-tuple-element.27), channel_id=1, source_target_pairs={{0,2},{2,4},{4,6},{6,0},{1,3},{3,5},{5,7},{7,1},{8,10},{10,12},{12... | collective-permute-start | bytes 393224 | tf_op jit(solution)/shard_map/ppermute | solution.py:17
  150.0 13.8 %collective-permute-start.9 = (bf16[32,2048]{0,1:T(8,128)(2,1)S(1)}, bf16[32,2048]{0,1:T(8,128)(2,1)S(1)}, u32[]{:S(2)}, u32[]{:S(2)}) collective-permute-start(bf16[32,2048]{0,1:T(8,128)(2,1)S(1)} %get-tuple-element.29), channel_id=1, source_target_pairs={{0,6},{2,0},{4,2},{6,4},{1,7},{3,1},{5,3},{7,5},{8,14},{10,8},{12,... | collective-permute-start | bytes 393224 | tf_op jit(solution)/shard_map/ppermute | solution.py:17
  164.4 14.3 %collective-permute-start.8 = (bf16[64,2048]{0,1:T(8,128)(2,1)S(1)}, bf16[64,2048]{0,1:T(8,128)(2,1)S(1)}, u32[]{:S(2)}, u32[]{:S(2)}) collective-permute-start(bf16[64,2048]{0,1:T(8,128)(2,1)S(1)} %pad_maximum_fusion.7), channel_id=1, source_target_pairs={{0,2},{2,4},{4,6},{6,0},{1,3},{3,5},{5,7},{7,1},{8,10},{10,12},{12... | collective-permute-start | bytes 786440 | tf_op jit(solution)/shard_map/ppermute | solution.py:17
  165.7 13.1 %collective-permute-start.10 = (bf16[64,2048]{0,1:T(8,128)(2,1)S(1)}, bf16[64,2048]{0,1:T(8,128)(2,1)S(1)}, u32[]{:S(2)}, u32[]{:S(2)}) collective-permute-start(bf16[64,2048]{0,1:T(8,128)(2,1)S(1)} %pad_maximum_fusion.8), channel_id=1, source_target_pairs={{0,6},{2,0},{4,2},{6,4},{1,7},{3,1},{5,3},{7,5},{8,14},{10,8},{12,... | collective-permute-start | bytes 786440 | tf_op jit(solution)/shard_map/ppermute | solution.py:17
  180.5 12.5 %collective-permute-start.12 = (bf16[64,2048]{0,1:T(8,128)(2,1)S(1)}, bf16[64,2048]{0,1:T(8,128)(2,1)S(1)}, u32[]{:S(2)}, u32[]{:S(2)}) collective-permute-start(bf16[64,2048]{0,1:T(8,128)(2,1)S(1)} %fusion.55), channel_id=1, source_target_pairs={{0,6},{2,0},{4,2},{6,4},{1,7},{3,1},{5,3},{7,5},{8,14},{10,8},{12,... | collective-permute-start | bytes 786440 | tf_op jit(solution)/shard_map/ppermute | solution.py:17
  183.3 14.2 %collective-permute-start.11 = (bf16[64,2048]{0,1:T(8,128)(2,1)S(1)}, bf16[64,2048]{0,1:T(8,128)(2,1)S(1)}, u32[]{:S(2)}, u32[]{:S(2)}) collective-permute-start(bf16[64,2048]{0,1:T(8,128)(2,1)S(1)} %fusion.55), channel_id=1, source_target_pairs={{0,2},{2,4},{4,6},{6,0},{1,3},{3,5},{5,7},{7,1},{8,10},{10,12},{12... | collective-permute-start | bytes 786440 | tf_op jit(solution)/shard_map/ppermute | solution.py:17
  194.0 12.8 %collective-permute-start.14 = (bf16[32,2048]{0,1:T(8,128)(2,1)}, bf16[32,2048]{0,1:T(8,128)(2,1)S(1)}, u32[]{:S(2)}, u32[]{:S(2)}) collective-permute-start(bf16[32,2048]{0,1:T(8,128)(2,1)} %slice.372), channel_id=1, source_target_pairs={{0,6},{2,0},{4,2},{6,4},{1,7},{3,1},{5,3},{7,5},{8,14},{10,8},{12,... | collective-permute-start | bytes 393224 | tf_op jit(solution)/shard_map/ppermute | solution.py:17
  198.3 12.4 %collective-permute-start.13 = (bf16[32,2048]{0,1:T(8,128)(2,1)}, bf16[32,2048]{0,1:T(8,128)(2,1)S(1)}, u32[]{:S(2)}, u32[]{:S(2)}) collective-permute-start(bf16[32,2048]{0,1:T(8,128)(2,1)} %bitcast.157), channel_id=1, source_target_pairs={{0,2},{2,4},{4,6},{6,0},{1,3},{3,5},{5,7},{7,1},{8,10},{10,12},{12... | collective-permute-start | bytes 393224 | tf_op jit(solution)/shard_map/ppermute | solution.py:17
  211.3 5.7 %collective-permute-start.15 = (bf16[4,64,2048]{2,1,0:T(8,128)(2,1)S(1)}, bf16[4,64,2048]{2,1,0:T(8,128)(2,1)S(1)}, u32[]{:S(2)}, u32[]{:S(2)}) collective-permute-start(bf16[4,64,2048]{2,1,0:T(8,128)(2,1)S(1)} %constant_dynamic-update-slice_fusion.1), channel_id=1, source_target_pairs={{0,1},{1,0},{2,3},{3,2},{4,5},{5,4},{6,7},{7,6},{8,9},{9,8},{10,11... | collective-permute-start | bytes 3145736 | tf_op jit(solution)/shard_map/ppermute | solution.py:17
  217.4 2.6 collective-permute-start.16
  231.4 3.7 %collective-permute-start.17 = (bf16[4,32,8,512]{3,2,1,0:T(8,128)(2,1)S(1)}, bf16[4,32,8,512]{3,2,1,0:T(8,128)(2,1)}, u32[]{:S(2)}, u32[]{:S(2)}) collective-permute-start(bf16[4,32,8,512]{3,2,1,0:T(8,128)(2,1)S(1)} %select_bitcast_fusion.3), channel_id=1, source_target_pairs={{0,1},{1,0},{2,3},{3,2},{4,5},{5,4},{6,7},{7,6},{8,9},{9,8},{10,11... | collective-permute-start | bytes 3145736 | tf_op jit(solution)/shard_map/ppermute | solution.py:17
  237.5 6.0 %collective-permute-start.18 = (bf16[16,8,512]{2,1,0:T(8,128)(2,1)S(1)}, bf16[16,8,512]{2,1,0:T(8,128)(2,1)S(1)}, u32[]{:S(2)}, u32[]{:S(2)}) collective-permute-start(bf16[16,8,512]{2,1,0:T(8,128)(2,1)S(1)} %get-tuple-element.37), channel_id=1, source_target_pairs={{0,2},{2,4},{4,6},{6,0},{1,3},{3,5},{5,7},{7,1},{8,10},{10,12},{12... | collective-permute-start | bytes 393224 | tf_op jit(solution)/shard_map/ppermute | solution.py:17
  238.1 5.3 %collective-permute-start.20 = (bf16[16,8,512]{2,1,0:T(8,128)(2,1)S(1)}, bf16[16,8,512]{2,1,0:T(8,128)(2,1)S(1)}, u32[]{:S(2)}, u32[]{:S(2)}) collective-permute-start(bf16[16,8,512]{2,1,0:T(8,128)(2,1)S(1)} %get-tuple-element.39), channel_id=1, source_target_pairs={{0,6},{2,0},{4,2},{6,4},{1,7},{3,1},{5,3},{7,5},{8,14},{10,8},{12,... | collective-permute-start | bytes 393224 | tf_op jit(solution)/shard_map/ppermute | solution.py:17
  243.6 20.7 %collective-permute-start.19 = (bf16[32,8,512]{2,1,0:T(8,128)(2,1)S(1)}, bf16[32,8,512]{2,1,0:T(8,128)(2,1)}, u32[]{:S(2)}, u32[]{:S(2)}) collective-permute-start(bf16[32,8,512]{2,1,0:T(8,128)(2,1)S(1)} %pad_maximum_fusion.11), channel_id=1, source_target_pairs={{0,2},{2,4},{4,6},{6,0},{1,3},{3,5},{5,7},{7,1},{8,10},{10,12},{12... | collective-permute-start | bytes 786440 | tf_op jit(solution)/shard_map/ppermute | solution.py:17
  244.7 19.6 %collective-permute-start.21 = (bf16[32,8,512]{2,1,0:T(8,128)(2,1)}, bf16[32,8,512]{2,1,0:T(8,128)(2,1)}, u32[]{:S(2)}, u32[]{:S(2)}) collective-permute-start(bf16[32,8,512]{2,1,0:T(8,128)(2,1)} %pad_maximum_fusion.12), channel_id=1, source_target_pairs={{0,6},{2,0},{4,2},{6,4},{1,7},{3,1},{5,3},{7,5},{8,14},{10,8},{12,... | collective-permute-start | bytes 786440 | tf_op jit(solution)/shard_map/ppermute | solution.py:17
  285.5 6.4 %collective-permute-start.22 = (bf16[8,16384]{1,0:T(8,128)(2,1)S(1)}, bf16[8,16384]{1,0:T(8,128)(2,1)S(1)}, u32[]{:S(2)}, u32[]{:S(2)}) collective-permute-start(bf16[8,16384]{1,0:T(8,128)(2,1)S(1)} %bitcast.153), channel_id=1, source_target_pairs={{0,2},{2,4},{4,6},{6,0},{1,3},{3,5},{5,7},{7,1},{8,10},{10,12},{12... | collective-permute-start | bytes 786440 | tf_op jit(solution)/shard_map/ppermute | solution.py:17
  285.5 6.6 %collective-permute-start.23 = (bf16[8,16384]{1,0:T(8,128)(2,1)S(1)}, bf16[8,16384]{1,0:T(8,128)(2,1)S(1)}, u32[]{:S(2)}, u32[]{:S(2)}) collective-permute-start(bf16[8,16384]{1,0:T(8,128)(2,1)S(1)} %bitcast.154), channel_id=1, source_target_pairs={{0,6},{2,0},{4,2},{6,4},{1,7},{3,1},{5,3},{7,5},{8,14},{10,8},{12,... | collective-permute-start | bytes 786440 | tf_op jit(solution)/shard_map/ppermute | solution.py:17
  292.0 5.6 %collective-permute-start.24 = (bf16[4,16384]{1,0:T(4,128)(2,1)S(1)}, bf16[4,16384]{1,0:T(4,128)(2,1)S(1)}, u32[]{:S(2)}, u32[]{:S(2)}) collective-permute-start(bf16[4,16384]{1,0:T(4,128)(2,1)S(1)} %slice.384), channel_id=1, source_target_pairs={{0,2},{2,4},{4,6},{6,0},{1,3},{3,5},{5,7},{7,1},{8,10},{10,12},{12... | collective-permute-start | bytes 393224 | tf_op jit(solution)/shard_map/ppermute | solution.py:17
  292.2 5.4 %collective-permute-start.25 = (bf16[4,16384]{1,0:T(4,128)(2,1)S(1)}, bf16[4,16384]{1,0:T(4,128)(2,1)S(1)}, u32[]{:S(2)}, u32[]{:S(2)}) collective-permute-start(bf16[4,16384]{1,0:T(4,128)(2,1)S(1)} %slice.385), channel_id=1, source_target_pairs={{0,6},{2,0},{4,2},{6,4},{1,7},{3,1},{5,3},{7,5},{8,14},{10,8},{12,... | collective-permute-start | bytes 393224 | tf_op jit(solution)/shard_map/ppermute | solution.py:17
  297.7 8.4 %collective-permute-start.26 = (bf16[4,8,16384]{2,1,0:T(8,128)(2,1)S(1)}, bf16[4,8,16384]{2,1,0:T(8,128)(2,1)S(1)}, u32[]{:S(2)}, u32[]{:S(2)}) collective-permute-start(bf16[4,8,16384]{2,1,0:T(8,128)(2,1)S(1)} %fusion.76), channel_id=1, source_target_pairs={{0,1},{1,0},{2,3},{3,2},{4,5},{5,4},{6,7},{7,6},{8,9},{9,8},{10,11... | collective-permute-start | bytes 3145736 | tf_op jit(solution)/shard_map/ppermute | solution.py:17
  (12 other events, 128.3 us)
Sparse Core Ops, SparseCore 0:
  10.7 106.4 all-gather.4
  119.8 100.2 all-gather.2
